TPU v7x, 256 devices: a whole 4x4x8 slice. The times are simulated.
256 devices in a mesh: sp: 16 (over y, x), tp: 16 (over z, core).
Axes of the slice: x: 4, y: 4, z: 8, core: 2. Of those that a mesh axis runs over, the one named last changes fastest.
Arguments:
- queries: bfloat16 [6144, 2048], P('sp', 'tp'), may hold values from -6 to 6
- keys: bfloat16 [6144, 2048], P('sp', 'tp'), may hold values from -6 to 6
- values: bfloat16 [6144, 2048], P('sp', 'tp'), may hold values from -6 to 6
- key_bias: bfloat16 [6144, 32], P('sp', 'tp'), may hold values from -16 to 0
- head_gain: float32 [32, 64], P('tp'), may hold values from 0.1 to 1.9
- out_weight: bfloat16 [2048, 2048], P('tp'), may hold values from -0.125 to 0.125
- residual: bfloat16 [6144, 2048], P(('sp', 'tp')), may hold values from -6 to 6
- norm_gain: float32 [2048], replicated, may hold values from 0.1 to 1.9
- gate_proj: bfloat16 [16, 2048, 7168], P('sp', None, 'tp'), may hold values from -0.125 to 0.125
- up_proj: bfloat16 [16, 2048, 7168], P('sp', None, 'tp'), may hold values from -0.125 to 0.125
- down_proj: bfloat16 [16, 7168, 2048], P('sp', 'tp'), may hold values from -0.0625 to 0.0625
- expert_choice: int32 [6144, 2], P(('sp', 'tp')), may hold values from 0 to 15, all different within a row; in each aligned block of 24 rows (0 to 23, 24 to 47, ...) at most 6 rows name the same one
- expert_weights: float32 [6144, 2], P(('sp', 'tp')), may hold values from 0.2 to 1
Outputs:
- layer_out: bfloat16 [6144, 2048], P(('sp', 'tp'))
Inputs may be any that keep to these rules, and one draw needn't show every extreme that they name: `expert_choice`: in each aligned block of 24 rows (the rows of one device), no expert is named more than 6 times; the two experts of a row differ.
All inputs are finite; a program needn't handle non-finite values.
Results may differ from a plain program's by a relative error of at most 0.019.
Values may be sent and summed in bfloat16 or wider, within the bound.
A program may use at most 128 MiB of HBM per device.

v0:
```python
import jax
import jax.numpy as jnp
from jax import lax
from jax.sharding import PartitionSpec as P

epsilon = 1e-06


def in_one_piece(arrays, axis, dim, along):
    ends, at = ([], 0)
    for a in arrays[:-1]:
        at += a.shape[along]
        ends.append(at)
    both = jnp.concatenate(arrays, axis=along)
    return tuple(jnp.split(lax.all_gather(both, axis, axis=dim, tiled=True), ends, axis=along))


def rms_scaled(values_in):
    return values_in * lax.rsqrt(jnp.mean(values_in * values_in, axis=-1, keepdims=True) + epsilon)


def expert_partial(row_block, gate_matrix, up_matrix, down_matrix):
    gate_part = jnp.dot(row_block, gate_matrix, preferred_element_type=jnp.float32)
    up_part = jnp.dot(row_block, up_matrix, preferred_element_type=jnp.float32)
    hidden = (jax.nn.silu(gate_part) * up_part).astype(jnp.bfloat16)
    return jnp.dot(hidden, down_matrix, preferred_element_type=jnp.float32)


def choice_ranks(routes, experts_all):
    flat_routes = routes.reshape(routes.shape[:-2] + (-1,))
    onehot = (flat_routes[..., None] == jnp.arange(experts_all, dtype=jnp.int32)).astype(jnp.int32)
    before = jnp.cumsum(onehot, axis=-2) - onehot
    return jnp.sum(before * onehot, axis=-1).reshape(routes.shape)


def slot_tokens(slot_index, targets, missing):
    flat_slots = slot_index.reshape(-1)
    owners = jnp.arange(flat_slots.shape[0], dtype=jnp.int32) // 2
    matches = flat_slots[None, :] == jnp.arange(targets, dtype=jnp.int32)[:, None]
    owner_found = jnp.sum(jnp.where(matches, owners[None, :], 0), axis=1)
    return jnp.where(jnp.any(matches, axis=1), owner_found, missing)


def on_device(
    queries,
    keys,
    values,
    key_bias,
    head_gain,
    out_weight,
    residual,
    norm_gain,
    gate_proj,
    up_proj,
    down_proj,
    expert_choice,
    expert_weights,
):
    rows_own = queries.shape[0]
    heads_here = head_gain.shape[0]
    head_size = head_gain.shape[1]
    model_width = out_weight.shape[1]
    seq_devices = lax.axis_size("sp")
    head_devices = lax.axis_size("tp")
    own_start = lax.axis_index("sp") * rows_own
    query_pos = own_start + jnp.arange(rows_own, dtype=jnp.int32)
    query_heads = queries.reshape(rows_own, heads_here, head_size)

    def key_block(slot_state, key_rows, value_rows, bias_rows, key_start):
        key_heads = key_rows.reshape(rows_own, heads_here, head_size)
        value_heads = value_rows.reshape(rows_own, heads_here, head_size)
        scores = jnp.einsum(
            "qhd,khd->hqk", query_heads, key_heads, preferred_element_type=jnp.float32
        ) * head_size ** (-0.5)
        scores = scores + bias_rows.astype(jnp.float32).T[:, None, :]
        key_pos = key_start + jnp.arange(rows_own, dtype=jnp.int32)
        earlier = (key_pos[None, :] < query_pos[:, None])[None, :, :]
        log_drops = jnp.where(earlier, jax.nn.log_sigmoid(-scores), 0.0)
        suffix = lax.cumsum(log_drops, axis=2, reverse=True) - log_drops
        within = jnp.where(earlier, jnp.exp(jax.nn.log_sigmoid(scores) + suffix), 0.0).astype(
            jnp.bfloat16
        )
        block_part = jnp.einsum(
            "hqk,khd->qhd", within, value_heads, preferred_element_type=jnp.float32
        )
        block_index = key_start // rows_own
        sums_new = lax.dynamic_update_index_in_dim(
            slot_state[0], block_part.reshape(rows_own, heads_here * head_size), block_index, 0
        )
        totals_new = lax.dynamic_update_index_in_dim(
            slot_state[1], jnp.sum(log_drops, axis=2), block_index, 0
        )
        return (sums_new, totals_new)

    empty_state = (
        jnp.zeros((seq_devices, rows_own, heads_here * head_size), jnp.float32),
        jnp.zeros((seq_devices, heads_here, rows_own), jnp.float32),
    )
    key_piece, value_piece, bias_piece = in_one_piece((keys, values, key_bias), "sp", 0, 1)

    def visit(block_count, state_in):
        offset = block_count * rows_own

        def take_rows(array):
            return lax.dynamic_slice_in_dim(array, offset, rows_own, 0)

        def compute(state_now):
            return key_block(
                state_now,
                take_rows(key_piece),
                take_rows(value_piece),
                take_rows(bias_piece),
                offset,
            )

        def keep(state_now):
            return state_now

        return lax.cond(offset <= own_start, compute, keep, state_in)

    block_sums, totals = lax.fori_loop(0, key_piece.shape[0] // rows_own, visit, empty_state)
    carried = jnp.sum(totals, axis=0, keepdims=True) - jnp.cumsum(totals, axis=0)
    factors = jnp.exp(carried).transpose(0, 2, 1)[..., None]
    mixture = jnp.sum(
        factors * block_sums.reshape(seq_devices, rows_own, heads_here, head_size), axis=0
    )
    attended = (
        (rms_scaled(mixture) * head_gain)
        .astype(jnp.bfloat16)
        .reshape(rows_own, heads_here * head_size)
    )
    row_share = rows_own // head_devices
    merged = lax.all_to_all(attended, "tp", split_axis=0, concat_axis=1, tiled=True)
    projected = jnp.dot(
        merged,
        lax.all_gather(out_weight, "tp", axis=0, tiled=True),
        preferred_element_type=jnp.float32,
    )
    stream = (residual.astype(jnp.float32) + projected).astype(jnp.bfloat16)
    normed = (rms_scaled(stream.astype(jnp.float32)) * norm_gain).astype(jnp.bfloat16)
    local_experts = gate_proj.shape[0]
    experts_all = local_experts * seq_devices
    capacity = 4 * rows_own // (head_devices * experts_all)
    own_slots = expert_choice * capacity + choice_ranks(expert_choice, experts_all)
    wanted = slot_tokens(own_slots, experts_all * capacity, row_share)
    outgoing = jnp.take(normed, wanted, axis=0, mode="fill", fill_value=0)
    arrived = lax.all_to_all(
        outgoing.reshape(seq_devices, local_experts, capacity, model_width),
        "sp",
        split_axis=0,
        concat_axis=0,
        tiled=True,
    )
    row_piece = lax.all_gather(arrived, "tp", axis=0, tiled=True)
    count_rows = row_piece.shape[0]
    partials = jnp.stack(
        [
            expert_partial(
                row_piece[:, 0].reshape(-1, model_width), gate_proj[0], up_proj[0], down_proj[0]
            ).reshape(count_rows, capacity, model_width)
        ],
        axis=1,
    )
    summed = lax.psum_scatter(partials.astype(jnp.bfloat16), "tp", scatter_dimension=0, tiled=True)
    returned = lax.all_to_all(summed, "sp", split_axis=0, concat_axis=0, tiled=True).reshape(
        experts_all * capacity, model_width
    )
    picked = jnp.take(returned, own_slots, axis=0).astype(jnp.float32)
    combined = jnp.sum(expert_weights[:, :, None] * picked, axis=1)
    return (stream.astype(jnp.float32) + combined).astype(jnp.bfloat16)


def solution(mesh):
    placed = (
        P("sp", "tp"),
        P("sp", "tp"),
        P("sp", "tp"),
        P("sp", "tp"),
        P("tp", None),
        P("tp", None),
        P(("sp", "tp"), None),
        P(),
        P("sp", None, "tp"),
        P("sp", None, "tp"),
        P("sp", "tp", None),
        P(("sp", "tp"), None),
        P(("sp", "tp"), None),
    )
    return jax.shard_map(
        on_device, mesh=mesh, in_specs=placed, out_specs=P(("sp", "tp"), None), check_vma=False
    )
```

profile of v0, /device:TPU:2, one launch (start us, length us, event | category | flops | bytes accessed | tf_op | source)
XLA Modules:
  0.0 624.2 jit_solution(17657157115760941867)
XLA Ops:
  15.2 55.1 %all-gather.4.cloned.1.call-done = bf16[6144,258]{0,1:T(8,128)(2,1)} async-done(((bf16[384,258]{0,1:T(8,128)(2,1)}), bf16[6144,258]{0,1:T(8,128)(2,1)}) %all-gather.4.cloned.1.call-update) | async-done | bytes 3170320 | tf_op jit(solution)/shard_map/all_gather | solution.py:15
  70.3 1.5 split.14
  71.8 3.9 fusion.30
  75.7 2.1 broadcast_in_dim.84
  78.4 41.8 %while.17 = (s32[]{:T(128)}, f32[16,384,128]{1,2,0:T(8,128)}, f32[16,2,384]{2,1,0:T(2,128)}, s32[]{:T(128)}, bf16[6144,128]{0,1:T(8,128)(2,1)}, /*index=5*/bf16[...) while((s32[]{:T(128)}, f32[16,384,128]{1,2,0:T(8,128)}, ...), condition=%wide.region_6.7_spmd.clone.clone, body=%wide.region_0.6_spmd.clone.clone.sunk | while | flops 122542848 | bytes 19914736 | solution.py:121
  78.4 20.5 %conditional.4 = ((f32[16,384,128]{1,2,0:T(8,128)}, f32[16,2,384]{2,1,0:T(2,128)})) conditional(s32[]{:T(128)} %convert_element_type.76, (f32[16,384,128]{1,2,0:T(8,128)}, f32[16,2,384]{2,1,0:T(2,128)}) %tuple.55, (s32[]{:T(128)}, bf16[6144,128]{0,1:T(8,128)(2,1)}, s32[]{:T(128)}, bf16[6144,128]{0,1:T(8,128)(2,1)}, bf16[384,2,64]{0,2,1:T(8,128)(2,1)}, ...), branch_computations={%region_1.0_spmd, %region_2.5_spmd} | conditional | flops 122542848 | bytes 19912984 | solution.py:119
  78.4 1.6 constant_dynamic-slice_fusion
  80.8 3.6 fusion.13
  84.4 7.0 %fusion.2 = f32[2,384,3,128]{1,2,3,0:T(4,128)S(1)} fusion(f32[2,384,3,128]{1,3,2,0:T(8,128)S(1)} %bitcast.71), kind=kOutput, calls=%fused_computation.5 | output fusion | flops 37453824 | bytes 2359296 | tf_op jit(solution)/shard_map/reduce-window
  95.7 1.6 fusion.10
  98.9 20.4 %conditional.4 = ((f32[16,384,128]{1,2,0:T(8,128)}, f32[16,2,384]{2,1,0:T(2,128)})) conditional(s32[]{:T(128)} %convert_element_type.76, (f32[16,384,128]{1,2,0:T(8,128)}, f32[16,2,384]{2,1,0:T(2,128)}) %tuple.55, (s32[]{:T(128)}, bf16[6144,128]{0,1:T(8,128)(2,1)}, s32[]{:T(128)}, bf16[6144,128]{0,1:T(8,128)(2,1)}, bf16[384,2,64]{0,2,1:T(8,128)(2,1)}, ...), branch_computations={%region_1.0_spmd, %region_2.5_spmd} | conditional | flops 122542848 | bytes 19912984 | solution.py:119
  98.9 1.6 constant_dynamic-slice_fusion
  101.4 3.6 fusion.13
  105.0 7.0 %fusion.2 = f32[2,384,3,128]{1,2,3,0:T(4,128)S(1)} fusion(f32[2,384,3,128]{1,3,2,0:T(8,128)S(1)} %bitcast.71), kind=kOutput, calls=%fused_computation.5 | output fusion | flops 37453824 | bytes 2359296 | tf_op jit(solution)/shard_map/reduce-window
  116.1 1.6 fusion.10
  121.9 2.2 fusion.14
  125.8 7.1 %all-to-all-start = ((bf16[16,24,128]{2,1,0:T(8,128)(2,1)}), bf16[16,24,128]{2,1,0:T(8,128)(2,1)S(1)}, u32[]{:S(2)}, u32[]{:S(2)}) async-start(bf16[16,24,128]{2,1,0:T(8,128)(2,1)} %multiply_convert_fusion.1), calls=%async_computation | async-start | bytes 196608 | tf_op jit(solution)/shard_map/all_to_all | solution.py:133
  133.0 8.2 %all-to-all-done = bf16[16,24,128]{2,1,0:T(8,128)(2,1)S(1)} async-done(((bf16[16,24,128]{2,1,0:T(8,128)(2,1)}), bf16[16,24,128]{2,1,0:T(8,128)(2,1)S(1)}, u32[]{:S(2)}, u32[]{:S(2)}) %all-to-all-start) | async-done | bytes 98336 | tf_op jit(solution)/shard_map/all_to_all | solution.py:133
  141.3 4.7 multiply_reduce_fusion.1
  148.0 300.1 %all_to_all.26 = bf16[16,1,6,2048]{3,2,1,0:T(8,128)(2,1)S(1)} all-to-all(bf16[16,1,6,2048]{3,2,1,0:T(8,128)(2,1)S(1)} %select_bitcast_fusion), channel_id=1, replica_groups=mesh['sp'=16,'tp'=16] {'sp'}, dimensions={0} | all-to-all | bytes 786432 | tf_op jit(solution)/shard_map/all_to_all | solution.py:147
  449.1 39.8 %all-gather.8.cloned.1.call-done = bf16[256,1,6,2048]{3,0,2,1:T(8,128)(2,1)} async-done(((bf16[16,1,6,2048]{3,0,2,1:T(8,128)(2,1)}), bf16[256,1,6,2048]{3,0,2,1:T(8,128)(2,1)}) %all-gather.8.cloned.1.call-update) | async-done | bytes 6291472 | tf_op jit(solution)/shard_map/all_gather | solution.py:154
  488.9 9.6 %copy.109 = bf16[256,1,6,2048]{3,2,0,1:T(8,128)(2,1)} copy(bf16[256,1,6,2048]{3,0,2,1:T(8,128)(2,1)} %all-gather.8.cloned.1.call-done) | data formatting | bytes 12582912 | tf_op jit(solution)/shard_map/all_gather | solution.py:154
  498.5 11.1 %reshape_squeeze.3 = bf16[1536,2048]{1,0:T(8,128)(2,1)} reshape(bf16[256,1,6,2048]{3,2,0,1:T(8,128)(2,1)} %copy.109) | data formatting | bytes 12582912 | tf_op jit(solution)/shard_map/reshape;squeeze | solution.py:159
  509.6 5.9 fusion.20
  515.5 4.3 fusion.15
  519.8 1.7 copy.110
  521.5 1.7 dot_general.23
  523.2 7.5 %convert_bitcast_fusion.1 = bf16[256,1,6,2048]{3,0,2,1:T(8,128)(2,1)} fusion(bf16[1,448,2048]{2,1,0:T(8,128)(2,1)S(1)} %copy-done, bf16[256,6,448]{2,1,0:T(8,128)(2,1)} %dot_general.23), kind=kOutput, calls=%fused_computation.29 | convolution fusion | flops 2821718016 | bytes 9502720 | tf_op jit(solution)/shard_map/dot_general | solution.py:26
  530.7 65.8 %reduce-scatter.2.cloned.1.call-done = bf16[16,1,6,2048]{3,0,2,1:T(8,128)(2,1)} async-done(((bf16[256,1,6,2048]{3,0,2,1:T(8,128)(2,1)}), bf16[16,1,6,2048]{3,0,2,1:T(8,128)(2,1)}) %reduce-scatter.2.cloned.1.call-update) | async-done | bytes 393232 | tf_op jit(solution)/shard_map/reduce_scatter | solution.py:164
  596.6 2.0 copy.112
  598.6 7.3 %all-to-all-start.2 = ((bf16[16,1,6,2048]{3,2,1,0:T(8,128)(2,1)}), bf16[16,1,6,2048]{3,2,1,0:T(8,128)(2,1)S(1)}, u32[]{:S(2)}, u32[]{:S(2)}) async-start(bf16[16,1,6,2048]{3,2,1,0:T(8,128)(2,1)} %copy.112), calls=%async_computation.3 | async-start | bytes 1048576 | tf_op jit(solution)/shard_map/all_to_all | solution.py:165
  606.3 8.4 %all-to-all-done.2 = bf16[16,1,6,2048]{3,2,1,0:T(8,128)(2,1)S(1)} async-done(((bf16[16,1,6,2048]{3,2,1,0:T(8,128)(2,1)}), bf16[16,1,6,2048]{3,2,1,0:T(8,128)(2,1)S(1)}, u32[]{:S(2)}, u32[]{:S(2)}) %all-to-all-start.2) | async-done | bytes 393248 | tf_op jit(solution)/shard_map/all_to_all | solution.py:165
  (154 shorter events, 32.4 us)
Async XLA Ops:
  6.5 516.7 %copy-start = (bf16[1,448,2048]{2,1,0:T(8,128)(2,1)S(1)}, bf16[1,448,2048]{2,1,0:T(8,128)(2,1)}, u32[]{:S(2)}) copy-start(bf16[1,448,2048]{2,1,0:T(8,128)(2,1)} %param.27) | copy-start | bytes 5505028
  6.5 4.4 copy-start.7
  6.5 5.1 copy-start.18
  6.5 5.7 copy-start.13
  6.5 63.7 %all-gather.4.cloned.1.call-start = ((), (), s32[]{:S(2)}) async-start(), calls=%async_computation.4 | async-start | bytes 3446784 | tf_op jit(solution)/shard_map/all_gather | solution.py:15
  10.1 131.1 %all-gather.6.cloned.1.call-start = ((), (), s32[]{:S(2)}) async-start(), calls=%async_computation.5 | async-start | bytes 8912896 | tf_op jit(solution)/shard_map/all_gather | solution.py:136
  13.5 62.2 %copy-start.10 = (s32[24,2]{0,1:T(2,128)}, s32[24,2]{0,1:T(2,128)S(1)}, u32[]{:S(2)}) copy-start(s32[24,2]{0,1:T(2,128)S(1)} %get-tuple-element.261) | copy-start | bytes 580
  94.3 1.3 copy-start.1
  94.4 2.9 copy-start.2
  95.7 2.6 copy-start.8
  114.9 1.3 copy-start.1
  115.0 2.8 copy-start.2
  116.1 2.6 copy-start.8
  124.1 1.1 copy-start.16
  124.1 8.9 %copy-start.9 = (s32[16,6]{1,0:T(8,128)S(1)}, s32[16,6]{1,0:T(8,128)}, u32[]{:S(2)}) copy-start(s32[16,6]{1,0:T(8,128)} %select_n.105) | copy-start | bytes 1156
  124.1 17.2 %copy-start.6 = (bf16[24,2048]{1,0:T(8,128)(2,1)S(1)}, bf16[24,2048]{1,0:T(8,128)(2,1)}, u32[]{:S(2)}) copy-start(bf16[24,2048]{1,0:T(8,128)(2,1)} %param.23) | copy-start | bytes 294916
  125.8 15.4 %all-to-all-start = ((bf16[16,24,128]{2,1,0:T(8,128)(2,1)}), bf16[16,24,128]{2,1,0:T(8,128)(2,1)S(1)}, u32[]{:S(2)}, u32[]{:S(2)}) async-start(bf16[16,24,128]{2,1,0:T(8,128)(2,1)} %multiply_convert_fusion.1), calls=%async_computation | async-start | bytes 196608 | tf_op jit(solution)/shard_map/all_to_all | solution.py:133
  132.9 356.0 %all-gather.8.cloned.1.call-start = ((), (), s32[]{:S(2)}) async-start(), calls=%async_computation.6 | async-start | bytes 6684672 | tf_op jit(solution)/shard_map/all_gather | solution.py:154
  133.0 13.6 %copy-start.12 = (f32[2048]{0:T(1024)S(1)}, f32[2048]{0:T(1024)}, u32[]{:S(2)}) copy-start(f32[2048]{0:T(1024)} %param.24) | copy-start | bytes 24580
  146.0 0.7 copy-start.4
  449.0 147.6 %reduce-scatter.2.cloned.1.call-start = ((), (), s32[]{:S(2)}) async-start(), calls=%async_computation.7 | async-start | bytes 6684672 | tf_op jit(solution)/shard_map/reduce_scatter | solution.py:164
  509.6 5.9 copy-start.3
  509.6 5.9 copy-start.17
  530.7 75.2 %copy-start.11 = (s32[24,2]{0,1:T(2,128)S(1)}, s32[24,2]{0,1:T(2,128)}, u32[]{:S(2)}) copy-start(s32[24,2]{0,1:T(2,128)} %copy-done.10) | copy-start | bytes 580
  530.7 75.4 %copy-start.14 = (pred[24,2]{0,1:T(4,128)(4,1)S(1)}, pred[24,2]{0,1:T(4,128)(4,1)}, u32[]{:S(2)}) copy-start(pred[24,2]{0,1:T(4,128)(4,1)} %get-tuple-element.260) | copy-start | bytes 148
  530.7 75.5 %copy-start.15 = (f32[24,2]{0,1:T(2,128)S(1)}, f32[24,2]{0,1:T(2,128)}, u32[]{:S(2)}) copy-start(f32[24,2]{0,1:T(2,128)} %param.29) | copy-start | bytes 580
  598.6 16.0 %all-to-all-start.2 = ((bf16[16,1,6,2048]{3,2,1,0:T(8,128)(2,1)}), bf16[16,1,6,2048]{3,2,1,0:T(8,128)(2,1)S(1)}, u32[]{:S(2)}, u32[]{:S(2)}) async-start(bf16[16,1,6,2048]{3,2,1,0:T(8,128)(2,1)} %copy.112), calls=%async_computation.3 | async-start | bytes 1048576 | tf_op jit(solution)/shard_map/all_to_all | solution.py:165
  606.3 10.8 %copy-start.5 = (f32[24,2048]{1,0:T(8,128)S(1)}, f32[24,2048]{1,0:T(8,128)}, u32[]{:S(2)}) copy-start(f32[24,2048]{1,0:T(8,128)} %copy-done.4) | copy-start | bytes 589828
Sparse Core Ops, SparseCore 0:
  10.3 59.9 all-gather.3
  72.1 55.5 all-gather.5
  449.2 39.7 all-gather.7
  530.8 65.7 reduce-scatter.1
where the time goes:
time: 629 us; the launch traced here: 624 us
  blocking collectives  300 us (48%)
  waiting for transfers between devices  178 us (28%)
  local copies, waits for them, and re-layouts  55 us (9%)
  other arithmetic  32.1 us (5%)
  matrix products  30 us (5%)
  starting transfers between devices  14.5 us (2%)
  between operations  13.5 us (2%)
    all_to_all x1, blocking collectives, on_device(): lax.all_to_all(outgoing.reshape(seq_devices, local_experts, capacity, mod...  300 us
    reduce_scatter x1, waiting for transfers between devices, on_device(): lax.psum_scatter(partials.astype(jnp.bfloat16), 'tp', scatter_dimension=0...  65.8 us
    all_gather x1, waiting for transfers between devices, in_one_piece(): lax.all_gather(both, axis, axis=dim, tiled=True)  55.1 us
    all_gather x1, waiting for transfers between devices, on_device(): row_piece = lax.all_gather(arrived, 'tp', axis=0, tiled=True)  39.8 us
    another operation x4, other arithmetic  16.6 us
  transfers between devices with their start and end apart: 6, of which 5 were waited for; matrix products, arithmetic and copies ran while one was open for 9% of the time, Pallas kernels for 0%

commit v1 on v0

--- a/solution.py
+++ b/solution.py
@@ -151,7 +151,9 @@
         concat_axis=0,
         tiled=True,
     )
-    row_piece = lax.all_gather(arrived, "tp", axis=0, tiled=True)
+    row_piece = jnp.concatenate(
+        lax.all_to_all(jnp.stack([arrived] * lax.axis_size("tp")), "tp", 0, 0), axis=0
+    )
     count_rows = row_piece.shape[0]
     partials = jnp.stack(
         [

time: 629 us -> 726 us (1.15)
  blocking collectives: 300 us -> 442 us
  waiting for transfers between devices: 178 us -> 135 us
    all_to_all x0 -> x1, blocking collectives: none -> 142 us  [on_device(): lax.all_to_all(jnp.stack([arrived] * lax.axis_size('tp')), 'tp', 0, 0)]
    all_gather x1 -> x0, waiting for transfers between devices: 39.8 us -> none  [on_device(): row_piece = lax.all_gather(arrived, 'tp', axis=0, tiled=True)]
    all_gather x1 -> x0, local copies, waits for them, and re-layouts: 9.6 us -> none  [on_device(): row_piece = lax.all_gather(arrived, 'tp', axis=0, tiled=True)]
    all_to_all x0 -> x1, local copies, waits for them, and re-layouts: none -> 7.62 us  [on_device(): lax.all_to_all(jnp.stack([arrived] * lax.axis_size('tp')), 'tp', 0, 0)]
  transfers between devices with their start and end apart: 6 -> 5, of which waited for: 5 -> 4; matrix products, arithmetic and copies ran while one was open for 9% -> 8% of each run, Pallas kernels for 0% -> 0%
where the time goes in v1:
time: 726 us; the launch traced here: 722 us
  blocking collectives  442 us (61%)
  waiting for transfers between devices  135 us (19%)
  local copies, waits for them, and re-layouts  53.1 us (7%)
  other arithmetic  32.1 us (4%)
  matrix products  30.1 us (4%)
  starting transfers between devices  14.5 us (2%)
  between operations  13.4 us (2%)
    all_to_all x1, blocking collectives, on_device(): lax.all_to_all(outgoing.reshape(seq_devices, local_experts, capacity, mod...  300 us
    all_to_all x1, blocking collectives, on_device(): lax.all_to_all(jnp.stack([arrived] * lax.axis_size('tp')), 'tp', 0, 0)  142 us
    reduce_scatter x1, waiting for transfers between devices, on_device(): lax.psum_scatter(partials.astype(jnp.bfloat16), 'tp', scatter_dimension=0...  62.8 us
    all_gather x1, waiting for transfers between devices, in_one_piece(): lax.all_gather(both, axis, axis=dim, tiled=True)  55 us
    another operation x4, other arithmetic  16.7 us
  transfers between devices with their start and end apart: 5, of which 4 were waited for; matrix products, arithmetic and copies ran while one was open for 8% of the time, Pallas kernels for 0%

profile of v1, /device:TPU:2, one launch (start us, length us, event | category | flops | bytes accessed | tf_op | source)
XLA Modules:
  0.0 721.9 jit_solution(3250621641956478856)
XLA Ops:
  15.2 55.0 %all-gather.3.cloned.1.call-done = bf16[6144,258]{0,1:T(8,128)(2,1)} async-done(((bf16[384,258]{0,1:T(8,128)(2,1)}), bf16[6144,258]{0,1:T(8,128)(2,1)}) %all-gather.3.cloned.1.call-update) | async-done | bytes 3170320 | tf_op jit(solution)/shard_map/all_gather | solution.py:15
  70.3 1.5 split.14
  71.8 3.9 fusion.30
  75.7 2.1 broadcast_in_dim.84
  78.4 41.8 %while.17 = (s32[]{:T(128)}, f32[16,384,128]{1,2,0:T(8,128)}, f32[16,2,384]{2,1,0:T(2,128)}, s32[]{:T(128)}, bf16[6144,128]{0,1:T(8,128)(2,1)}, /*index=5*/bf16[...) while((s32[]{:T(128)}, f32[16,384,128]{1,2,0:T(8,128)}, ...), condition=%wide.region_6.7_spmd.clone.clone, body=%wide.region_0.6_spmd.clone.clone.sunk | while | flops 122542848 | bytes 19914736 | solution.py:121
  78.4 20.5 %conditional.4 = ((f32[16,384,128]{1,2,0:T(8,128)}, f32[16,2,384]{2,1,0:T(2,128)})) conditional(s32[]{:T(128)} %convert_element_type.76, (f32[16,384,128]{1,2,0:T(8,128)}, f32[16,2,384]{2,1,0:T(2,128)}) %tuple.55, (s32[]{:T(128)}, bf16[6144,128]{0,1:T(8,128)(2,1)}, s32[]{:T(128)}, bf16[6144,128]{0,1:T(8,128)(2,1)}, bf16[384,2,64]{0,2,1:T(8,128)(2,1)}, ...), branch_computations={%region_1.0_spmd, %region_2.5_spmd} | conditional | flops 122542848 | bytes 19912984 | solution.py:119
  78.4 1.6 constant_dynamic-slice_fusion
  80.9 3.6 fusion.13
  84.5 7.0 fusion.2
  95.7 1.6 fusion.10
  98.9 20.4 %conditional.4 = ((f32[16,384,128]{1,2,0:T(8,128)}, f32[16,2,384]{2,1,0:T(2,128)})) conditional(s32[]{:T(128)} %convert_element_type.76, (f32[16,384,128]{1,2,0:T(8,128)}, f32[16,2,384]{2,1,0:T(2,128)}) %tuple.55, (s32[]{:T(128)}, bf16[6144,128]{0,1:T(8,128)(2,1)}, s32[]{:T(128)}, bf16[6144,128]{0,1:T(8,128)(2,1)}, bf16[384,2,64]{0,2,1:T(8,128)(2,1)}, ...), branch_computations={%region_1.0_spmd, %region_2.5_spmd} | conditional | flops 122542848 | bytes 19912984 | solution.py:119
  98.9 1.6 constant_dynamic-slice_fusion
  101.4 3.6 fusion.13
  105.0 7.0 fusion.2
  116.1 1.6 fusion.10
  121.9 2.2 fusion.14
  125.8 7.1 all-to-all-start
  133.1 8.2 %all-to-all-done = bf16[16,24,128]{2,1,0:T(8,128)(2,1)S(1)} async-done(((bf16[16,24,128]{2,1,0:T(8,128)(2,1)}), bf16[16,24,128]{2,1,0:T(8,128)(2,1)S(1)}, u32[]{:S(2)}, u32[]{:S(2)}) %all-to-all-start) | async-done | bytes 98336 | tf_op jit(solution)/shard_map/all_to_all | solution.py:133
  141.3 4.7 multiply_reduce_fusion.1
  148.0 300.3 %all_to_all.34 = bf16[16,1,6,2048]{3,2,1,0:T(8,128)(2,1)S(1)} all-to-all(bf16[16,1,6,2048]{3,2,1,0:T(8,128)(2,1)S(1)} %select_bitcast_fusion), channel_id=1, replica_groups=mesh['sp'=16,'tp'=16] {'sp'}, dimensions={0} | all-to-all | bytes 786432 | tf_op jit(solution)/shard_map/all_to_all | solution.py:147
  449.3 142.2 %all_to_all.35 = bf16[16,16,1,6,2048]{4,1,3,2,0:T(8,128)(2,1)S(1)} all-to-all(bf16[16,16,1,6,2048]{4,1,3,2,0:T(8,128)(2,1)S(1)} %stack.2), channel_id=1, replica_groups=mesh['sp'=16,'tp'=16] {'tp'}, dimensions={0} | all-to-all | bytes 12582912 | tf_op jit(solution)/shard_map/all_to_all | solution.py:155
  591.5 7.6 %copy.109 = bf16[16,16,1,6,2048]{4,3,1,0,2:T(8,128)(2,1)} copy(bf16[16,16,1,6,2048]{4,1,3,2,0:T(8,128)(2,1)S(1)} %all_to_all.35) | data formatting | bytes 12582912 | tf_op jit(solution)/shard_map/all_to_all | solution.py:155
  599.1 11.0 %reshape_squeeze_reshape.3 = bf16[1536,2048]{1,0:T(8,128)(2,1)} reshape(bf16[16,16,1,6,2048]{4,3,1,0,2:T(8,128)(2,1)} %copy.109) | data formatting | bytes 12582912 | tf_op jit(solution)/shard_map/reshape;squeeze;reshape | solution.py:161
  610.2 6.0 fusion.20
  616.2 4.3 fusion.15
  620.5 1.7 copy.110
  622.2 1.7 dot_general.23
  623.9 7.5 %convert_bitcast_fusion.1 = bf16[256,1,6,2048]{3,0,2,1:T(8,128)(2,1)} fusion(bf16[1,448,2048]{2,1,0:T(8,128)(2,1)S(1)} %copy-done, bf16[256,6,448]{2,1,0:T(8,128)(2,1)} %dot_general.23), kind=kOutput, calls=%fused_computation.29 | convolution fusion | flops 2821718016 | bytes 9502720 | tf_op jit(solution)/shard_map/dot_general | solution.py:26
  631.4 62.8 %reduce-scatter.2.cloned.1.call-done = bf16[16,1,6,2048]{3,0,2,1:T(8,128)(2,1)} async-done(((bf16[256,1,6,2048]{3,0,2,1:T(8,128)(2,1)}), bf16[16,1,6,2048]{3,0,2,1:T(8,128)(2,1)}) %reduce-scatter.2.cloned.1.call-update) | async-done | bytes 393232 | tf_op jit(solution)/shard_map/reduce_scatter | solution.py:166
  694.2 2.0 copy.112
  696.2 7.3 %all-to-all-start.3 = ((bf16[16,1,6,2048]{3,2,1,0:T(8,128)(2,1)}), bf16[16,1,6,2048]{3,2,1,0:T(8,128)(2,1)S(1)}, u32[]{:S(2)}, u32[]{:S(2)}) async-start(bf16[16,1,6,2048]{3,2,1,0:T(8,128)(2,1)} %copy.112), calls=%async_computation.4 | async-start | bytes 1048576 | tf_op jit(solution)/shard_map/all_to_all | solution.py:167
  703.9 8.4 %all-to-all-done.3 = bf16[16,1,6,2048]{3,2,1,0:T(8,128)(2,1)S(1)} async-done(((bf16[16,1,6,2048]{3,2,1,0:T(8,128)(2,1)}), bf16[16,1,6,2048]{3,2,1,0:T(8,128)(2,1)S(1)}, u32[]{:S(2)}, u32[]{:S(2)}) %all-to-all-start.3) | async-done | bytes 393248 | tf_op jit(solution)/shard_map/all_to_all | solution.py:167
  (153 shorter events, 32.4 us)
Async XLA Ops:
  6.5 617.3 %copy-start = (bf16[1,448,2048]{2,1,0:T(8,128)(2,1)S(1)}, bf16[1,448,2048]{2,1,0:T(8,128)(2,1)}, u32[]{:S(2)}) copy-start(bf16[1,448,2048]{2,1,0:T(8,128)(2,1)} %param.27) | copy-start | bytes 5505028
  6.5 4.4 copy-start.7
  6.5 5.1 copy-start.18
  6.5 5.8 copy-start.13
  6.5 63.7 %all-gather.3.cloned.1.call-start = ((), (), s32[]{:S(2)}) async-start(), calls=%async_computation.5 | async-start | bytes 3446784 | tf_op jit(solution)/shard_map/all_gather | solution.py:15
  10.1 131.1 %all-gather.5.cloned.1.call-start = ((), (), s32[]{:S(2)}) async-start(), calls=%async_computation.6 | async-start | bytes 8912896 | tf_op jit(solution)/shard_map/all_gather | solution.py:136
  13.6 62.2 %copy-start.10 = (s32[24,2]{0,1:T(2,128)}, s32[24,2]{0,1:T(2,128)S(1)}, u32[]{:S(2)}) copy-start(s32[24,2]{0,1:T(2,128)S(1)} %get-tuple-element.261) | copy-start | bytes 580
  94.4 1.3 copy-start.1
  94.5 2.9 copy-start.2
  95.7 2.6 copy-start.8
  114.9 1.3 copy-start.1
  115.0 2.8 copy-start.2
  116.1 2.6 copy-start.8
  124.1 1.1 copy-start.16
  124.1 8.9 %copy-start.9 = (s32[16,6]{1,0:T(8,128)S(1)}, s32[16,6]{1,0:T(8,128)}, u32[]{:S(2)}) copy-start(s32[16,6]{1,0:T(8,128)} %select_n.105) | copy-start | bytes 1156
  124.1 17.2 %copy-start.6 = (bf16[24,2048]{1,0:T(8,128)(2,1)S(1)}, bf16[24,2048]{1,0:T(8,128)(2,1)}, u32[]{:S(2)}) copy-start(bf16[24,2048]{1,0:T(8,128)(2,1)} %param.23) | copy-start | bytes 294916
  125.8 15.4 %all-to-all-start = ((bf16[16,24,128]{2,1,0:T(8,128)(2,1)}), bf16[16,24,128]{2,1,0:T(8,128)(2,1)S(1)}, u32[]{:S(2)}, u32[]{:S(2)}) async-start(bf16[16,24,128]{2,1,0:T(8,128)(2,1)} %multiply_convert_fusion.1), calls=%async_computation | async-start | bytes 196608 | tf_op jit(solution)/shard_map/all_to_all | solution.py:133
  133.0 561.2 %reduce-scatter.2.cloned.1.call-start = ((), (), s32[]{:S(2)}) async-start(), calls=%async_computation.7 | async-start | bytes 6684672 | tf_op jit(solution)/shard_map/reduce_scatter | solution.py:166
  133.0 13.6 %copy-start.12 = (f32[2048]{0:T(1024)S(1)}, f32[2048]{0:T(1024)}, u32[]{:S(2)}) copy-start(f32[2048]{0:T(1024)} %param.24) | copy-start | bytes 24580
  146.0 0.7 copy-start.4
  610.2 6.0 copy-start.3
  610.2 6.0 copy-start.17
  631.4 72.1 %copy-start.11 = (s32[24,2]{0,1:T(2,128)S(1)}, s32[24,2]{0,1:T(2,128)}, u32[]{:S(2)}) copy-start(s32[24,2]{0,1:T(2,128)} %copy-done.10) | copy-start | bytes 580
  631.4 72.3 %copy-start.14 = (pred[24,2]{0,1:T(4,128)(4,1)S(1)}, pred[24,2]{0,1:T(4,128)(4,1)}, u32[]{:S(2)}) copy-start(pred[24,2]{0,1:T(4,128)(4,1)} %get-tuple-element.260) | copy-start | bytes 148
  631.4 72.4 %copy-start.15 = (f32[24,2]{0,1:T(2,128)S(1)}, f32[24,2]{0,1:T(2,128)}, u32[]{:S(2)}) copy-start(f32[24,2]{0,1:T(2,128)} %param.29) | copy-start | bytes 580
  696.2 16.1 %all-to-all-start.3 = ((bf16[16,1,6,2048]{3,2,1,0:T(8,128)(2,1)}), bf16[16,1,6,2048]{3,2,1,0:T(8,128)(2,1)S(1)}, u32[]{:S(2)}, u32[]{:S(2)}) async-start(bf16[16,1,6,2048]{3,2,1,0:T(8,128)(2,1)} %copy.112), calls=%async_computation.4 | async-start | bytes 1048576 | tf_op jit(solution)/shard_map/all_to_all | solution.py:167
  703.9 10.8 %copy-start.5 = (f32[24,2048]{1,0:T(8,128)S(1)}, f32[24,2048]{1,0:T(8,128)}, u32[]{:S(2)}) copy-start(f32[24,2048]{1,0:T(8,128)} %copy-done.4) | copy-start | bytes 589828
Sparse Core Ops, SparseCore 0:
  10.3 59.9 all-gather.2
  72.1 55.5 all-gather.4
  631.5 62.6 reduce-scatter.1
